TPU v7x, 32 devices: a whole 2x2x4 slice. The times are simulated.
32 devices in a mesh: ep: 8 (over z, y), tp: 4 (over x, core).
Axes of the slice: x: 2, y: 2, z: 4, core: 2. Of those that a mesh axis runs over, the one named last changes fastest.
Arguments:
- tokens: bfloat16 [1024, 2048], P('ep'), may hold values from -6 to 6
- norm_gain: float32 [2048], replicated, may hold values from 0.1 to 1.9
- routes: int32 [1024, 2], P('ep'), may hold values from 0 to 7, all different within a row; in each aligned block of 128 rows (0 to 127, 128 to 255, ...) at most 48 rows name the same one
- group_prob: float32 [1024], P('ep'), may hold values from 0.2 to 1
- expert_logits: float32 [1024, 2], P('ep'), may hold values from -6 to 6
- gate_weight: bfloat16 [8, 2048, 384], P('ep', None, 'tp'), may hold values from -0.125 to 0.125
- up_weight: bfloat16 [8, 2048, 384], P('ep', None, 'tp'), may hold values from -0.125 to 0.125
- down_matrix: bfloat16 [8, 384, 2048], P('ep', 'tp'), may hold values from -0.3125 to 0.3125
Outputs:
- combined: bfloat16 [1024, 2048], P('ep', 'tp')
Inputs may be any that keep to these rules, and one draw needn't show every extreme that they name: `routes`: each row names 2 different experts. Among the 128 tokens of one index of ep at most 48 rows name one expert, and in every draw some expert is named by exactly 48 of them.
All inputs are finite; a program needn't handle non-finite values.
Results may differ from a plain program's by a relative error of at most 0.013.
Values may be sent and summed in bfloat16 or wider, within the bound.
A program may use at most 64 MiB of HBM per device.

v0:
```python
import jax
import jax.numpy as jnp
from jax import lax
from jax.sharding import PartitionSpec as P


def hidden_part(buffer, gate_weight, up_weight):
    local_count = gate_weight.shape[0]
    grouped = buffer.reshape(
        buffer.shape[0] // local_count, local_count, buffer.shape[1], buffer.shape[2]
    )
    gate_proj = jnp.einsum(
        "sknd,kdf->sknf", grouped, gate_weight, preferred_element_type=jnp.float32
    )
    up_proj = jnp.einsum("sknd,kdf->sknf", grouped, up_weight, preferred_element_type=jnp.float32)
    hidden_state = (jax.nn.silu(gate_proj) * up_proj).astype(jnp.bfloat16)
    return hidden_state.reshape(buffer.shape[0], buffer.shape[1], hidden_state.shape[3])


def down_blocks(hidden_full, down_cols, block_count):
    local_count = down_cols.shape[0]
    width = hidden_full.shape[2] // block_count
    grouped = hidden_full.reshape(
        hidden_full.shape[0] // local_count, local_count, hidden_full.shape[1], block_count, width
    )
    columns = down_cols.reshape(local_count, block_count, width, down_cols.shape[2])
    block_list = jnp.einsum(
        "sknrf,krfd->sknrd", grouped, columns, preferred_element_type=jnp.float32
    ).astype(jnp.bfloat16)
    summed = jnp.sum(block_list.astype(jnp.float32), 3).astype(jnp.bfloat16)
    return summed.reshape(hidden_full.shape[0], hidden_full.shape[1], down_cols.shape[2])


def body(tokens, norm_gain, routes, group_prob, expert_logits, gate_weight, up_weight, down_matrix):
    tok_rows, model_width = tokens.shape
    top_count = routes.shape[1]
    experts = gate_weight.shape[0] * lax.axis_size("ep")
    capacity = 3 * top_count * tok_rows // (2 * experts)
    block_count = lax.axis_size("tp")
    down_cols = lax.all_to_all(down_matrix, "tp", split_axis=2, concat_axis=1, tiled=True)
    values = tokens.astype(jnp.float32)
    normed = (
        values * lax.rsqrt(jnp.mean(values * values, -1, keepdims=True) + 1e-06) * norm_gain
    ).astype(jnp.bfloat16)
    flat_ids = routes.reshape(-1)
    onehot = (flat_ids[:, None] == jnp.arange(experts, dtype=jnp.int32)[None, :]).astype(jnp.int32)
    earlier = jnp.cumsum(onehot, 0) - onehot
    slot_index = jnp.sum(earlier * onehot, 1)
    target = flat_ids * capacity + slot_index
    owners = jnp.arange(tok_rows * top_count, dtype=jnp.int32) // top_count
    outgoing = (
        jnp.zeros((experts * capacity, model_width), jnp.bfloat16).at[target].set(normed[owners])
    )
    outgoing = outgoing.reshape(experts, capacity, model_width)
    hidden_state = hidden_part(
        lax.all_to_all(outgoing, "ep", split_axis=0, concat_axis=0, tiled=True),
        gate_weight,
        up_weight,
    )
    hidden_full = lax.all_gather(hidden_state, "tp", axis=2, tiled=True)
    summed = down_blocks(hidden_full, down_cols, block_count)
    returned = lax.all_to_all(summed, "ep", split_axis=0, concat_axis=0, tiled=True)
    flat_back = returned.reshape(experts * capacity, returned.shape[2])
    weights = group_prob[:, None] * jax.nn.softmax(expert_logits, axis=-1)
    picked = flat_back[target].reshape(tok_rows, top_count, flat_back.shape[1]).astype(jnp.float32)
    combined = jnp.sum(picked * weights[:, :, None], 1).astype(jnp.bfloat16)
    return combined


def solution(mesh):
    return jax.shard_map(
        body,
        mesh=mesh,
        in_specs=(
            P("ep", None),
            P(),
            P("ep", None),
            P("ep"),
            P("ep", None),
            P("ep", None, "tp"),
            P("ep", None, "tp"),
            P("ep", "tp", None),
        ),
        out_specs=P("ep", "tp"),
        check_vma=False,
    )
```

profile of v0, /device:TPU:0, one launch (start us, length us, event | category | flops | bytes accessed | tf_op | source)
XLA Modules:
  0.0 104.3 jit_solution(11414660805682031129)
XLA Ops:
  0.0 2.4 %copy.32 = bf16[1,96,2048]{1,0,2:T(2,128)(2,1)S(1)} copy(bf16[1,96,2048]{2,1,0:T(8,128)(2,1)} %param.15) | data formatting | bytes 786432 | tf_op args[7]
  2.4 0.5 broadcast.137
  2.9 11.6 %reduce.6 = bf16[2048,96]{1,0:T(8,128)(2,1)S(1)} reduce(bf16[2048,1,96]{2,1,0:T(2,128)(2,1)S(1)} %bitcast.53, bf16[]{:T(256)} %broadcast.137), dimensions={1}, to_apply=%bitcast.44.reduce_sub_computation | reduce | bytes 786434
  14.5 1.6 %reshape.188 = bf16[4,2,24576]{2,1,0:T(2,128)(2,1)} reshape(bf16[2048,96]{1,0:T(8,128)(2,1)S(1)} %reduce.6) | data formatting | bytes 786432
  16.1 4.2 %all-to-all-start = ((bf16[4,2,24576]{2,1,0:T(2,128)(2,1)}), bf16[4,2,24576]{2,1,0:T(2,128)(2,1)S(1)}, u32[]{:S(2)}, u32[]{:S(2)}) async-start(bf16[4,2,24576]{2,1,0:T(2,128)(2,1)} %reshape.188), calls=%async_computation | async-start | bytes 786432 | tf_op jit(solution)/shard_map/all_to_all | solution.py:40
  20.4 0.1 eq.29
  20.6 0.1 eq.25
  20.7 0.6 reduce-window.6
  21.3 0.2 slice_reduce_fusion
  21.7 0.1 mul.63
  21.9 0.2 fusion.2
  22.2 0.2 fusion.4
  22.4 6.7 %scatter_custom_fusion = bf16[384,2048]{1,0:T(8,128)(2,1)} fusion(s32[256]{0:T(256)S(1)} %bitcast.57, bf16[128,2048]{1,0:T(8,128)(2,1)S(1)} %fusion.4, s32[1024]{0:T(1024)S(1)} %pad_clamp_fusion.1, bf16[]{:T(256)} %constant.32.clone.1), kind=kCustom, calls=%fused_computation.13 | custom fusion | bytes 1572866 | tf_op jit(solution)/shard_map/scatter | solution.py:52
  29.1 6.7 %all-to-all-start.1 = ((bf16[8,48,2048]{2,1,0:T(8,128)(2,1)}), bf16[8,48,2048]{2,1,0:T(8,128)(2,1)S(1)}, u32[]{:S(2)}, u32[]{:S(2)}) async-start(bf16[8,48,2048]{2,1,0:T(8,128)(2,1)} %bitcast.6), calls=%async_computation.1 | async-start | bytes 3145728 | tf_op jit(solution)/shard_map/all_to_all | solution.py:56
  35.9 0.8 reshape.189
  36.6 1.9 %fusion.14 = (bf16[1,96,512]{1,0,2:T(2,128)(2,1)}, bf16[1,96,512]{1,0,2:T(2,128)(2,1)S(1)}, bf16[1,96,512]{1,0,2:T(2,128)(2,1)S(1)}, bf16[1,96,512]{1,0,2:T(2,128)(2,1)}) fusion(bf16[1,96,2048]{1,0,2:T(2,128)(2,1)S(1)} %bitcast.52), kind=kLoop, calls=%fused_computation.40 | loop fusion | bytes 786432 | tf_op jit(solution)/shard_map/slice.2
  38.5 1.1 %copy.33 = bf16[1,96,512]{2,1,0:T(8,128)(2,1)S(1)} copy(bf16[1,96,512]{1,0,2:T(2,128)(2,1)} %get-tuple-element.5) | data formatting | bytes 196608 | tf_op jit(solution)/shard_map/slice.2
  39.6 1.1 %copy.34 = bf16[1,96,512]{2,1,0:T(8,128)(2,1)S(1)} copy(bf16[1,96,512]{1,0,2:T(2,128)(2,1)} %get-tuple-element.8) | data formatting | bytes 196608 | tf_op jit(solution)/shard_map/slice.3
  40.7 0.1 copy.35
  41.0 32.3 %all-to-all-done.1 = bf16[8,48,2048]{2,1,0:T(8,128)(2,1)S(1)} async-done(((bf16[8,48,2048]{2,1,0:T(8,128)(2,1)}), bf16[8,48,2048]{2,1,0:T(8,128)(2,1)S(1)}, u32[]{:S(2)}, u32[]{:S(2)}) %all-to-all-start.1) | async-done | bytes 1572896 | tf_op jit(solution)/shard_map/all_to_all | solution.py:56
  73.3 0.6 convolution_bitcast_fusion.1
  73.9 0.6 fusion.1
  74.5 0.2 copy.40
  74.6 8.7 %all-gather = bf16[8,1,48,384]{2,0,1,3:T(8,128)(2,1)S(1)} all-gather(bf16[8,1,48,96]{2,0,1,3:T(8,128)(2,1)S(1)} %copy.40), channel_id=2, replica_groups=mesh['ep'=8,'tp'=4] {'tp'}, dimensions={3}, use_global_device_ids=true | all-gather | bytes 368640 | tf_op jit(solution)/shard_map/all_gather | solution.py:60
  83.4 0.5 copy.42
  83.9 0.5 fusion.15
  84.4 1.1 %convert_reduce_fusion = bf16[512,8,48]{0,2,1:T(8,128)(2,1)} fusion(f32[4,512,8,48]{1,3,2,0:T(8,128)S(1)} %bitcast.51), kind=kLoop, calls=%fused_computation.3 | loop fusion | flops 1376256 | bytes 3538944 | tf_op jit(solution)/shard_map/reduce_sum | solution.py:30
  85.6 3.6 %all-to-all-start.2 = ((bf16[8,48,512]{2,1,0:T(8,128)(2,1)}), bf16[8,48,512]{2,1,0:T(8,128)(2,1)S(1)}, u32[]{:S(2)}, u32[]{:S(2)}) async-start(bf16[8,48,512]{2,1,0:T(8,128)(2,1)} %bitcast.23), calls=%async_computation.2 | async-start | bytes 786432 | tf_op jit(solution)/shard_map/all_to_all | solution.py:62
  89.4 12.0 %all-to-all-done.2 = bf16[8,48,512]{2,1,0:T(8,128)(2,1)S(1)} async-done(((bf16[8,48,512]{2,1,0:T(8,128)(2,1)}), bf16[8,48,512]{2,1,0:T(8,128)(2,1)S(1)}, u32[]{:S(2)}, u32[]{:S(2)}) %all-to-all-start.2) | async-done | bytes 393248 | tf_op jit(solution)/shard_map/all_to_all | solution.py:62
  101.4 1.2 %gather_fusion = bf16[256,512]{1,0:T(8,128)(2,1)S(1)} fusion(bf16[384,512]{1,0:T(8,128)(2,1)S(1)} %bitcast.50, s32[1024]{0:T(1024)S(1)} %pad_clamp_fusion), kind=kCustom, calls=%fused_computation.1 | custom fusion | bytes 525312 | tf_op jit(solution)/shard_map/gather | solution.py:65
  102.6 0.3 reshape.150
  102.9 1.4 %multiply_reduce_fusion = bf16[128,512]{1,0:T(8,128)(2,1)} fusion(f32[128,2,512]{2,1,0:T(2,128)S(1)} %reshape.150, f32[128,2]{1,0:T(8,128)S(1)} %copy.43), kind=kLoop, calls=%fused_computation.16 | loop fusion | flops 196608 | bytes 656384 | tf_op jit(solution)/shard_map/reduce_sum | solution.py:66
  (33 shorter events, 0.8 us)
Async XLA Ops:
  0.0 73.3 %copy-start = (bf16[1,2048,96]{1,2,0:T(8,128)(2,1)S(1)}, bf16[1,2048,96]{1,2,0:T(8,128)(2,1)}, u32[]{:S(2)}) copy-start(bf16[1,2048,96]{1,2,0:T(8,128)(2,1)} %param.13) | copy-start | bytes 1179652
  2.9 17.4 %copy-start.4 = (s32[128,2]{0,1:T(2,128)S(1)}, s32[128,2]{0,1:T(2,128)}, u32[]{:S(2)}) copy-start(s32[128,2]{0,1:T(2,128)} %param.10) | copy-start | bytes 3076
  2.9 19.0 %copy-start.1 = (bf16[128,2048]{1,0:T(8,128)(2,1)S(1)}, bf16[128,2048]{1,0:T(8,128)(2,1)}, u32[]{:S(2)}) copy-start(bf16[128,2048]{1,0:T(8,128)(2,1)} %param.8) | copy-start | bytes 1572868
  14.5 7.6 %copy-start.3 = (f32[2048]{0:T(1024)S(1)}, f32[2048]{0:T(1024)}, u32[]{:S(2)}) copy-start(f32[2048]{0:T(1024)} %param.9) | copy-start | bytes 24580
  16.1 13.1 %all-to-all-start = ((bf16[4,2,24576]{2,1,0:T(2,128)(2,1)}), bf16[4,2,24576]{2,1,0:T(2,128)(2,1)S(1)}, u32[]{:S(2)}, u32[]{:S(2)}) async-start(bf16[4,2,24576]{2,1,0:T(2,128)(2,1)} %reshape.188), calls=%async_computation | async-start | bytes 786432 | tf_op jit(solution)/shard_map/all_to_all | solution.py:40
  29.1 44.2 %all-to-all-start.1 = ((bf16[8,48,2048]{2,1,0:T(8,128)(2,1)}), bf16[8,48,2048]{2,1,0:T(8,128)(2,1)S(1)}, u32[]{:S(2)}, u32[]{:S(2)}) async-start(bf16[8,48,2048]{2,1,0:T(8,128)(2,1)} %bitcast.6), calls=%async_computation.1 | async-start | bytes 3145728 | tf_op jit(solution)/shard_map/all_to_all | solution.py:56
  40.9 33.0 %copy-start.6 = (bf16[1,2048,96]{1,2,0:T(8,128)(2,1)S(1)}, bf16[1,2048,96]{1,2,0:T(8,128)(2,1)}, u32[]{:S(2)}) copy-start(bf16[1,2048,96]{1,2,0:T(8,128)(2,1)} %param.14) | copy-start | bytes 1179652
  84.4 4.8 %copy-start.2 = (f32[128,2]{0,1:T(2,128)S(1)}, f32[128,2]{0,1:T(2,128)}, u32[]{:S(2)}) copy-start(f32[128,2]{0,1:T(2,128)} %param.12) | copy-start | bytes 3076
  84.4 4.8 %copy-start.5 = (f32[128]{0:T(128)S(1)}, f32[128]{0:T(128)}, u32[]{:S(2)}) copy-start(f32[128]{0:T(128)} %param.11) | copy-start | bytes 1540
  85.6 15.9 %all-to-all-start.2 = ((bf16[8,48,512]{2,1,0:T(8,128)(2,1)}), bf16[8,48,512]{2,1,0:T(8,128)(2,1)S(1)}, u32[]{:S(2)}, u32[]{:S(2)}) async-start(bf16[8,48,512]{2,1,0:T(8,128)(2,1)} %bitcast.23), calls=%async_computation.2 | async-start | bytes 786432 | tf_op jit(solution)/shard_map/all_to_all | solution.py:62
where the time goes:
time: 105 us; the launch traced here: 104 us
  waiting for transfers between devices  44.4 us (42%)
  local copies, waits for them, and re-layouts  19.4 us (18%)
  other arithmetic  15.3 us (15%)
  starting transfers between devices  14.6 us (14%)
  blocking collectives  8.74 us (8%)
  matrix products  1.68 us (2%)
    all_to_all x1, waiting for transfers between devices, body(): lax.all_to_all(outgoing, 'ep', split_axis=0, concat_axis=0, tiled=True)  32.3 us
    all_to_all x1, waiting for transfers between devices, body(): lax.all_to_all(summed, 'ep', split_axis=0, concat_axis=0, tiled=True)  12 us
    unnamed x1, other arithmetic  11.6 us
    all_gather x1, blocking collectives, body(): hidden_full = lax.all_gather(hidden_state, 'tp', axis=2, tiled=True)  8.74 us
    scatter x1, local copies, waits for them, and re-layouts, body(): jnp.zeros((experts * capacity, model_width), jnp.bfloat16).at[target]  6.74 us
    all_to_all x1, starting transfers between devices, body(): lax.all_to_all(outgoing, 'ep', split_axis=0, concat_axis=0, tiled=True)  6.73 us
    unnamed x19, local copies, waits for them, and re-layouts  5.36 us
    another operation x7, local copies, waits for them, and re-layouts  4.77 us
  transfers between devices with their start and end apart: 3, of which 2 were waited for; matrix products, arithmetic and copies ran while one was open for 13% of the time, Pallas kernels for 0%

commit v1 on v0

--- a/solution.py
+++ b/solution.py
@@ -57,7 +57,12 @@
         gate_weight,
         up_weight,
     )
-    hidden_full = lax.all_gather(hidden_state, "tp", axis=2, tiled=True)
+    ring = [hidden_state]
+    for hop in range(3):
+        ring.append(lax.ppermute(ring[-1], "tp", [(dev, (dev + 1) % 4) for dev in range(4)]))
+    hidden_full = jnp.roll(
+        jnp.concatenate(ring[::-1], axis=2), (lax.axis_index("tp") + 1) * ring[0].shape[2], axis=2
+    )
     summed = down_blocks(hidden_full, down_cols, block_count)
     returned = lax.all_to_all(summed, "ep", split_axis=0, concat_axis=0, tiled=True)
     flat_back = returned.reshape(experts * capacity, returned.shape[2])

time: 105 us -> 96.3 us (0.917)
  blocking collectives: 8.74 us -> 0 us
  local copies, waits for them, and re-layouts: 19.4 us -> 16 us
  other arithmetic: 15.3 us -> 18 us
    all_to_all x1, waiting for transfers between devices: 32.3 us -> 22.6 us  [body(): lax.all_to_all(outgoing, 'ep', split_axis=0, concat_axis=0, tiled=True)]
    all_gather x1 -> x0, blocking collectives: 8.74 us -> none  [body(): hidden_full = lax.all_gather(hidden_state, 'tp', axis=2, tiled=True)]
    ppermute x0 -> x3, waiting for transfers between devices: none -> 6.44 us  [body(): lax.ppermute(ring[-1], 'tp', [(dev, (dev + 1) % 4) for dev in range(4)])]
    all_to_all x1, waiting for transfers between devices: 0.01 us -> 6.27 us  [body(): lax.all_to_all(down_matrix, 'tp', split_axis=2, concat_axis=1, tiled=True)]
    another operation x7 -> x8, local copies, waits for them, and re-layouts: 4.77 us -> 1.88 us
    all_to_all x1, waiting for transfers between devices: 12 us -> 9.41 us  [body(): lax.all_to_all(summed, 'ep', split_axis=0, concat_axis=0, tiled=True)]
    unnamed x19 -> x15, local copies, waits for them, and re-layouts: 5.36 us -> 4.46 us
  transfers between devices with their start and end apart: 3 -> 6, of which waited for: 2 -> 5; matrix products, arithmetic and copies ran while one was open for 13% -> 19% of each run, Pallas kernels for 0% -> 0%
where the time goes in v1:
time: 96.3 us; the launch traced here: 95.8 us
  waiting for transfers between devices  44.7 us (46%)
  other arithmetic  18 us (19%)
  local copies, waits for them, and re-layouts  16 us (17%)
  starting transfers between devices  15.1 us (16%)
  matrix products  1.68 us (2%)
    all_to_all x1, waiting for transfers between devices, body(): lax.all_to_all(outgoing, 'ep', split_axis=0, concat_axis=0, tiled=True)  22.6 us
    unnamed x1, other arithmetic  11.5 us
    all_to_all x1, waiting for transfers between devices, body(): lax.all_to_all(summed, 'ep', split_axis=0, concat_axis=0, tiled=True)  9.41 us
    all_to_all x1, starting transfers between devices, body(): lax.all_to_all(outgoing, 'ep', split_axis=0, concat_axis=0, tiled=True)  7.44 us
    scatter x1, local copies, waits for them, and re-layouts, body(): jnp.zeros((experts * capacity, model_width), jnp.bfloat16).at[target]  6.74 us
    ppermute x3, waiting for transfers between devices, body(): lax.ppermute(ring[-1], 'tp', [(dev, (dev + 1) % 4) for dev in range(4)])  6.44 us
    all_to_all x1, waiting for transfers between devices, body(): lax.all_to_all(down_matrix, 'tp', split_axis=2, concat_axis=1, tiled=True)  6.27 us
    unnamed x15, local copies, waits for them, and re-layouts  4.46 us
  transfers between devices with their start and end apart: 6, of which 5 were waited for; matrix products, arithmetic and copies ran while one was open for 19% of the time, Pallas kernels for 0%

profile of v1, /device:TPU:0, one launch (start us, length us, event | category | flops | bytes accessed | tf_op | source)
XLA Modules:
  0.0 95.8 jit_solution(1577492573152358375)
XLA Ops:
  0.0 0.8 copy.28
  1.1 0.7 broadcast_multiply_fusion
  1.8 0.6 reduce-window.6
  2.4 0.2 slice_reduce_fusion
  2.9 1.2 %fusion.3 = f32[128]{0:T(128)S(1)} fusion(bf16[128,2048]{1,0:T(8,128)(2,1)} %param.8), kind=kLoop, calls=%fused_computation.11 | loop fusion | flops 786304 | bytes 524800 | tf_op jit(solution)/shard_map/reduce_sum | solution.py:43
  4.3 1.2 %fusion.5 = bf16[128,2048]{1,0:T(8,128)(2,1)S(1)} fusion(bf16[128,2048]{1,0:T(8,128)(2,1)} %param.8, f32[2048]{0:T(1024)} %param.9, f32[128]{0:T(128)S(1)} %add_rsqrt_fusion), kind=kLoop, calls=%fused_computation.13 | loop fusion | flops 1048576 | bytes 1057280 | tf_op jit(solution)/shard_map/convert_element_type | solution.py:44
  5.5 6.7 %scatter_custom_fusion = bf16[384,2048]{1,0:T(8,128)(2,1)} fusion(s32[256]{0:T(256)S(1)} %bitcast.59, bf16[128,2048]{1,0:T(8,128)(2,1)S(1)} %fusion.5, s32[1024]{0:T(1024)S(1)} %pad_clamp_fusion.1, bf16[]{:T(256)} %constant.53.clone.1), kind=kCustom, calls=%fused_computation.14 | custom fusion | bytes 1572866 | tf_op jit(solution)/shard_map/scatter | solution.py:52
  12.3 7.4 %all-to-all-start.1 = ((bf16[8,48,2048]{2,1,0:T(8,128)(2,1)}), bf16[8,48,2048]{2,1,0:T(8,128)(2,1)S(1)}, u32[]{:S(2)}, u32[]{:S(2)}) async-start(bf16[8,48,2048]{2,1,0:T(8,128)(2,1)} %bitcast.6), calls=%async_computation.1 | async-start | bytes 3145728 | tf_op jit(solution)/shard_map/all_to_all | solution.py:56
  19.7 0.8 copy.22
  20.5 0.5 broadcast.141
  21.0 11.5 %reduce.6 = bf16[2048,96]{1,0:T(8,128)(2,1)S(1)} reduce(bf16[2048,1,96]{2,1,0:T(2,128)(2,1)S(1)} %bitcast.56, bf16[]{:T(256)} %broadcast.141), dimensions={1}, to_apply=%bitcast.47.reduce_sub_computation | reduce | bytes 786434
  32.5 1.6 %reshape.186 = bf16[4,2,24576]{2,1,0:T(2,128)(2,1)} reshape(bf16[2048,96]{1,0:T(8,128)(2,1)S(1)} %reduce.6) | data formatting | bytes 786432
  34.1 22.6 %all-to-all-done.1 = bf16[8,48,2048]{2,1,0:T(8,128)(2,1)S(1)} async-done(((bf16[8,48,2048]{2,1,0:T(8,128)(2,1)}), bf16[8,48,2048]{2,1,0:T(8,128)(2,1)S(1)}, u32[]{:S(2)}, u32[]{:S(2)}) %all-to-all-start.1) | async-done | bytes 1572896 | tf_op jit(solution)/shard_map/all_to_all | solution.py:56
  56.7 3.5 %all-to-all-start = ((bf16[4,2,24576]{2,1,0:T(2,128)(2,1)}), bf16[4,2,24576]{2,1,0:T(2,128)(2,1)S(1)}, u32[]{:S(2)}, u32[]{:S(2)}) async-start(bf16[4,2,24576]{2,1,0:T(2,128)(2,1)} %reshape.186), calls=%async_computation | async-start | bytes 786432 | tf_op jit(solution)/shard_map/all_to_all | solution.py:40
  60.2 0.6 convolution_bitcast_fusion.1
  60.8 0.6 fusion.2
  61.3 0.5 collective-permute-start
  61.9 6.3 %all-to-all-done = bf16[4,2,24576]{2,1,0:T(2,128)(2,1)S(1)} async-done(((bf16[4,2,24576]{2,1,0:T(2,128)(2,1)}), bf16[4,2,24576]{2,1,0:T(2,128)(2,1)S(1)}, u32[]{:S(2)}, u32[]{:S(2)}) %all-to-all-start) | async-done | bytes 393248 | tf_op jit(solution)/shard_map/all_to_all | solution.py:40
  68.1 0.8 reshape.187
  69.0 1.1 %fusion.15 = (bf16[1,96,512]{1,0,2:T(2,128)(2,1)S(1)}, bf16[1,96,512]{1,0,2:T(2,128)(2,1)S(1)}, bf16[1,96,512]{1,0,2:T(2,128)(2,1)S(1)}, bf16[1,96,512]{1,0,2:T(2,128)(2,1)S(1)}) fusion(bf16[1,96,2048]{1,0,2:T(2,128)(2,1)S(1)} %bitcast.55), kind=kLoop, calls=%fused_computation.42 | loop fusion | bytes 786432 | tf_op jit(solution)/shard_map/slice.2
  70.6 2.4 %collective-permute-done.1 = bf16[8,48,96]{2,1,0:T(8,128)(2,1)S(1)} collective-permute-done((bf16[8,48,96]{2,1,0:T(8,128)(2,1)S(1)}, bf16[8,48,96]{2,1,0:T(8,128)(2,1)S(1)}, u32[]{:S(2)}, u32[]{:S(2)}) %collective-permute-start.1) | collective-permute-done | bytes 73760 | tf_op jit(solution)/shard_map/ppermute | solution.py:62
  73.0 4.0 %collective-permute-done.2 = bf16[8,48,96]{2,1,0:T(8,128)(2,1)S(1)} collective-permute-done((bf16[8,48,96]{2,1,0:T(8,128)(2,1)S(1)}, bf16[8,48,96]{2,1,0:T(8,128)(2,1)S(1)}, u32[]{:S(2)}, u32[]{:S(2)}) %collective-permute-start.2) | collective-permute-done | bytes 73760 | tf_op jit(solution)/shard_map/ppermute | solution.py:62
  77.0 0.5 concatenate.10
  77.5 0.2 constant_dynamic-slice_fusion
  77.7 0.3 reshape.148
  78.0 0.5 fusion.16
  78.6 1.1 %convert_reduce_fusion = bf16[512,8,48]{0,2,1:T(8,128)(2,1)} fusion(f32[4,512,8,48]{1,3,2,0:T(8,128)S(1)} %bitcast.54), kind=kLoop, calls=%fused_computation.3 | loop fusion | flops 1376256 | bytes 3538944 | tf_op jit(solution)/shard_map/reduce_sum | solution.py:30
  79.7 3.6 %all-to-all-start.2 = ((bf16[8,48,512]{2,1,0:T(8,128)(2,1)}), bf16[8,48,512]{2,1,0:T(8,128)(2,1)S(1)}, u32[]{:S(2)}, u32[]{:S(2)}) async-start(bf16[8,48,512]{2,1,0:T(8,128)(2,1)} %bitcast.23), calls=%async_computation.2 | async-start | bytes 786432 | tf_op jit(solution)/shard_map/all_to_all | solution.py:67
  83.6 9.4 %all-to-all-done.2 = bf16[8,48,512]{2,1,0:T(8,128)(2,1)S(1)} async-done(((bf16[8,48,512]{2,1,0:T(8,128)(2,1)}), bf16[8,48,512]{2,1,0:T(8,128)(2,1)S(1)}, u32[]{:S(2)}, u32[]{:S(2)}) %all-to-all-start.2) | async-done | bytes 393248 | tf_op jit(solution)/shard_map/all_to_all | solution.py:67
  93.0 1.2 %gather_fusion = bf16[256,512]{1,0:T(8,128)(2,1)S(1)} fusion(bf16[384,512]{1,0:T(8,128)(2,1)S(1)} %bitcast.53, s32[1024]{0:T(1024)S(1)} %pad_clamp_fusion), kind=kCustom, calls=%fused_computation.1 | custom fusion | bytes 525312 | tf_op jit(solution)/shard_map/gather | solution.py:70
  94.1 0.3 reshape.150
  94.5 1.4 %multiply_reduce_fusion = bf16[128,512]{1,0:T(8,128)(2,1)} fusion(f32[128,2,512]{2,1,0:T(2,128)S(1)} %reshape.150, f32[128,2]{1,0:T(8,128)S(1)} %copy.31), kind=kLoop, calls=%fused_computation.17 | loop fusion | flops 196608 | bytes 656384 | tf_op jit(solution)/shard_map/reduce_sum | solution.py:71
  (36 shorter events, 1.5 us)
Async XLA Ops:
  0.0 60.2 %copy-start = (bf16[1,2048,96]{1,2,0:T(8,128)(2,1)S(1)}, bf16[1,2048,96]{1,2,0:T(8,128)(2,1)}, u32[]{:S(2)}) copy-start(bf16[1,2048,96]{1,2,0:T(8,128)(2,1)} %param.13) | copy-start | bytes 1179652
  12.3 7.4 %copy-start.1 = (bf16[1,96,2048]{2,1,0:T(8,128)(2,1)S(1)}, bf16[1,96,2048]{2,1,0:T(8,128)(2,1)}, u32[]{:S(2)}) copy-start(bf16[1,96,2048]{2,1,0:T(8,128)(2,1)} %param.15) | copy-start | bytes 1179652
  12.3 44.4 %all-to-all-start.1 = ((bf16[8,48,2048]{2,1,0:T(8,128)(2,1)}), bf16[8,48,2048]{2,1,0:T(8,128)(2,1)S(1)}, u32[]{:S(2)}, u32[]{:S(2)}) async-start(bf16[8,48,2048]{2,1,0:T(8,128)(2,1)} %bitcast.6), calls=%async_computation.1 | async-start | bytes 3145728 | tf_op jit(solution)/shard_map/all_to_all | solution.py:56
  34.1 26.7 %copy-start.4 = (bf16[1,2048,96]{1,2,0:T(8,128)(2,1)S(1)}, bf16[1,2048,96]{1,2,0:T(8,128)(2,1)}, u32[]{:S(2)}) copy-start(bf16[1,2048,96]{1,2,0:T(8,128)(2,1)} %param.14) | copy-start | bytes 1179652
  56.7 11.4 %all-to-all-start = ((bf16[4,2,24576]{2,1,0:T(2,128)(2,1)}), bf16[4,2,24576]{2,1,0:T(2,128)(2,1)S(1)}, u32[]{:S(2)}, u32[]{:S(2)}) async-start(bf16[4,2,24576]{2,1,0:T(2,128)(2,1)} %reshape.186), calls=%async_computation | async-start | bytes 786432 | tf_op jit(solution)/shard_map/all_to_all | solution.py:40
  61.3 7.6 %collective-permute-start = (bf16[8,48,96]{2,1,0:T(8,128)(2,1)S(1)}, bf16[8,48,96]{2,1,0:T(8,128)(2,1)S(1)}, u32[]{:S(2)}, u32[]{:S(2)}) collective-permute-start(bf16[8,48,96]{2,1,0:T(8,128)(2,1)S(1)} %fusion.2), channel_id=1, source_target_pairs={{0,1},{1,2},{2,3},{3,0},{4,5},{5,6},{6,7},{7,4},{8,9},{9,10},{10,1... | collective-permute-start | bytes 221192 | tf_op jit(solution)/shard_map/ppermute | solution.py:62
  68.9 4.1 %collective-permute-start.1 = (bf16[8,48,96]{2,1,0:T(8,128)(2,1)S(1)}, bf16[8,48,96]{2,1,0:T(8,128)(2,1)S(1)}, u32[]{:S(2)}, u32[]{:S(2)}) collective-permute-start(bf16[8,48,96]{2,1,0:T(8,128)(2,1)S(1)} %collective-permute-done), channel_id=1, source_target_pairs={{0,1},{1,2},{2,3},{3,0},{4,5},{5,6},{6,7},{7,4},{8,9},{9,10},{10,1... | collective-permute-start | bytes 221192 | tf_op jit(solution)/shard_map/ppermute | solution.py:62
  73.0 4.0 %collective-permute-start.2 = (bf16[8,48,96]{2,1,0:T(8,128)(2,1)S(1)}, bf16[8,48,96]{2,1,0:T(8,128)(2,1)S(1)}, u32[]{:S(2)}, u32[]{:S(2)}) collective-permute-start(bf16[8,48,96]{2,1,0:T(8,128)(2,1)S(1)} %collective-permute-done.1), channel_id=1, source_target_pairs={{0,1},{1,2},{2,3},{3,0},{4,5},{5,6},{6,7},{7,4},{8,9},{9,10},{10,1... | collective-permute-start | bytes 221192 | tf_op jit(solution)/shard_map/ppermute | solution.py:62
  78.6 4.8 %copy-start.2 = (f32[128,2]{0,1:T(2,128)S(1)}, f32[128,2]{0,1:T(2,128)}, u32[]{:S(2)}) copy-start(f32[128,2]{0,1:T(2,128)} %param.12) | copy-start | bytes 3076
  78.6 4.8 %copy-start.3 = (f32[128]{0:T(128)S(1)}, f32[128]{0:T(128)}, u32[]{:S(2)}) copy-start(f32[128]{0:T(128)} %param.11) | copy-start | bytes 1540
  79.7 13.2 %all-to-all-start.2 = ((bf16[8,48,512]{2,1,0:T(8,128)(2,1)}), bf16[8,48,512]{2,1,0:T(8,128)(2,1)S(1)}, u32[]{:S(2)}, u32[]{:S(2)}) async-start(bf16[8,48,512]{2,1,0:T(8,128)(2,1)} %bitcast.23), calls=%async_computation.2 | async-start | bytes 786432 | tf_op jit(solution)/shard_map/all_to_all | solution.py:67
